TPU v7x, 32 devices: a whole 2x2x4 slice. The times are simulated.
32 devices in a mesh: grp: 2 (over y), ep: 4 (over z), tp: 4 (over x, core).
Axes of the slice: x: 2, y: 2, z: 4, core: 2. Of those that a mesh axis runs over, the one named last changes fastest.
Arguments:
- mix_input: bfloat16 [2048, 2048], P(('grp', 'ep'), 'tp'), parts along dimension 0, may hold values from -6 to 6
- group_weight: bfloat16 [16, 128, 128], replicated, may hold values from -0.5 to 0.5
- pool_gain: float32 [2048], replicated, may hold values from 0.1 to 1.9
- branch_weight: bfloat16 [2048, 2048], P('tp'), may hold values from -0.125 to 0.125
- exp_input: bfloat16 [1024, 2048], P(('grp', 'ep')), parts along dimension 0, may hold values from -6 to 6
- norm_gain: float32 [2048], replicated, may hold values from 0.1 to 1.9
- routes: int32 [1024, 2], P(('grp', 'ep')), parts along dimension 0, may hold values from 0 to 3, all different within a row; in each aligned block of 128 rows (0 to 127, 128 to 255, ...) at most 96 rows name the same one
- route_weights: float32 [1024, 2], P(('grp', 'ep')), parts along dimension 0, may hold values from 0.25 to 1
- gate_weight: bfloat16 [4, 2048, 3584], P('ep', None, 'tp'), may hold values from -0.125 to 0.125
- up_weight: bfloat16 [4, 2048, 3584], P('ep', None, 'tp'), may hold values from -0.125 to 0.125
- down_weight: bfloat16 [4, 3584, 2048], P('ep', 'tp'), may hold values from -0.09375 to 0.09375
Outputs:
- mix_out: bfloat16 [2048, 2048], P(('grp', 'ep'), 'tp'), parts along dimension 0
- exp_out: bfloat16 [1024, 2048], P(('grp', 'ep'), 'tp'), parts along dimension 0
There are 2 independent parts, one for each index of `grp`. A program takes and returns all parts, laid end to end along the dimension named above; an argument that names none is the same for every part. Nothing has to cross between parts.
Inputs may be any that keep to these rules, and one draw needn't show every extreme that they name: `routes`: the 2 experts of a token differ. Among the 128 tokens of one index of ep no expert is named by more than 96 of them, a bound that some block reaches.
All inputs are finite; a program needn't handle non-finite values.
Results may differ from a plain program's by a relative error of at most 0.018.
Values may be sent and summed in bfloat16 or wider, within the bound.
No kernel may reach another device: no remote copies, remote signals or barrier semaphores. Data moves between devices by JAX's collectives and lax.ppermute only.
A program may use at most 64 MiB of HBM per device.

v0:
```python
import jax
import jax.numpy as jnp
from jax import lax
from jax.sharding import PartitionSpec as P

windows = (2, 4, 8, 16)
epsilon = 1e-06


def shifted(block, axis, distance):
    devices = range(lax.axis_size(axis))
    route = [(i - distance, i) for i in devices if i - distance in devices]
    return lax.ppermute(block, axis, route)


def trailing_sums(extended, rows):
    span_two = extended[1:] + extended[:-1]
    span_four = span_two[2:] + span_two[:-2]
    span_eight = span_four[4:] + span_four[:-4]
    span_sixteen = span_eight[8:] + span_eight[:-8]
    return [span_two[-rows:], span_four[-rows:], span_eight[-rows:], span_sixteen]


def pooled_deviation(extended, positions, group_ids, group_width, rows):
    sums = trailing_sums(extended, rows)
    current = extended[-rows:]
    window_id = jnp.repeat(group_ids % 4, group_width)
    result = jnp.zeros_like(current)
    for window_level, window_len in enumerate(windows):
        counted = jnp.minimum(positions + 1, window_len).astype(jnp.float32)[:, None]
        result = jnp.where(
            window_id[None, :] == window_level, sums[window_level] / counted - current, result
        )
    return result


def on_device(
    mix_input,
    group_weight,
    pool_gain,
    branch_weight,
    exp_input,
    norm_gain,
    routes,
    route_weights,
    gate_weight,
    up_weight,
    down_weight,
):
    tp_rank = lax.axis_index("tp")
    ep_rank = lax.axis_index("ep")
    rows_mix, channels = mix_input.shape
    group_width = group_weight.shape[1]
    group_count = channels // group_width
    first_group = tp_rank * group_count
    last_rows = mix_input[rows_mix - 15 :]
    before = shifted(last_rows, "ep", 1)
    extended = jnp.concatenate([before, mix_input], axis=0).astype(jnp.float32)
    positions = ep_rank * rows_mix + jnp.arange(rows_mix, dtype=jnp.int32)
    group_ids = first_group + jnp.arange(group_count, dtype=jnp.int32)
    deviation = pooled_deviation(extended, positions, group_ids, group_width, rows_mix).astype(
        jnp.bfloat16
    )
    own_groups = lax.dynamic_slice_in_dim(group_weight, first_group, group_count, 0)
    grouped = jnp.einsum(
        "rgc,gcd->rgd",
        deviation.reshape(rows_mix, group_count, group_width),
        own_groups,
        preferred_element_type=jnp.float32,
    ).reshape(rows_mix, channels)
    own_gain = lax.dynamic_slice_in_dim(pool_gain, first_group * group_width, channels, 0)
    pooled = (grouped * own_gain).astype(jnp.bfloat16)
    tok_rows, width = exp_input.shape
    columns = width // lax.axis_size("tp")
    experts_all = lax.axis_size("ep")
    capacity = 3 * tok_rows // experts_all
    floated = exp_input.astype(jnp.float32)
    normed = (
        floated
        * lax.rsqrt(jnp.mean(floated * floated, axis=1, keepdims=True) + epsilon)
        * norm_gain
    ).astype(jnp.bfloat16)
    flat_expert = routes.reshape(-1)
    assignments = flat_expert.shape[0]
    onehot = (flat_expert[:, None] == jnp.arange(experts_all, dtype=jnp.int32)[None, :]).astype(
        jnp.int32
    )
    slot_rank = jnp.sum((jnp.cumsum(onehot, axis=0) - onehot) * onehot, axis=1)
    slot_index = flat_expert * capacity + slot_rank
    token_of = jnp.arange(assignments, dtype=jnp.int32) // routes.shape[1]
    slot_token = (
        jnp.full((experts_all * capacity,), tok_rows, jnp.int32).at[slot_index].set(token_of)
    )
    padded = jnp.concatenate([normed, jnp.zeros((1, width), jnp.bfloat16)], axis=0)
    w_gate = gate_weight[0]
    w_up = up_weight[0]
    w_down = down_weight[0]
    arrived_rows = experts_all * capacity
    own_columns = lax.dynamic_slice_in_dim(padded, tp_rank * columns, columns, 1)
    outgoing = own_columns[slot_token].reshape(experts_all, capacity, columns)
    arrived = lax.all_to_all(outgoing, "ep", split_axis=0, concat_axis=0, tiled=True).reshape(
        arrived_rows, columns
    )
    section = lax.all_gather(arrived, "tp", axis=1, tiled=True)
    gate_pre = jnp.dot(section, w_gate, preferred_element_type=jnp.float32)
    up_pre = jnp.dot(section, w_up, preferred_element_type=jnp.float32)
    hidden = (jax.nn.silu(gate_pre) * up_pre).astype(jnp.bfloat16)
    weight_cols = branch_weight
    mix_sum = lax.psum_scatter(
        lax.dot_general(
            weight_cols, pooled, (((0,), (1,)), ((), ())), preferred_element_type=jnp.float32
        ).astype(jnp.bfloat16),
        "tp",
        scatter_dimension=0,
        tiled=True,
    )
    weight_cols = w_down
    exp_sum = lax.psum_scatter(
        lax.dot_general(
            weight_cols, hidden, (((0,), (1,)), ((), ())), preferred_element_type=jnp.float32
        ).astype(jnp.bfloat16),
        "tp",
        scatter_dimension=0,
        tiled=True,
    )
    mix_out = mix_sum.T
    results = exp_sum.reshape(columns, experts_all, capacity)
    returned = lax.all_to_all(results, "ep", split_axis=1, concat_axis=1, tiled=True).reshape(
        columns, experts_all * capacity
    )
    picked = returned[:, slot_index].astype(jnp.float32)
    weighted = picked * route_weights.reshape(-1)[None, :]
    combined = jnp.sum(weighted.reshape(columns, tok_rows, routes.shape[1]), axis=2)
    exp_out = combined.T.astype(jnp.bfloat16)
    return (mix_out, exp_out)


def solution(mesh):
    return jax.shard_map(
        on_device,
        mesh=mesh,
        in_specs=(
            P(("grp", "ep"), "tp"),
            P(),
            P(),
            P("tp", None),
            P(("grp", "ep"), None),
            P(),
            P(("grp", "ep"), None),
            P(("grp", "ep"), None),
            P("ep", None, "tp"),
            P("ep", None, "tp"),
            P("ep", "tp", None),
        ),
        out_specs=(P(("grp", "ep"), "tp"), P(("grp", "ep"), "tp")),
        check_vma=False,
    )
```

profile of v0, /device:TPU:0, one launch (start us, length us, event | category | flops | bytes accessed | tf_op | source)
XLA Modules:
  0.0 130.7 jit_solution(4550041975561271826)
XLA Ops:
  7.2 0.9 copy.21
  8.3 0.1 eq.93
  8.4 0.7 broadcast_multiply_fusion
  9.1 1.2 fusion.19
  10.4 1.2 reduce-window.6
  12.1 0.1 mul.84
  12.3 1.4 %scatter_custom_fusion = s32[384]{0:T(512)S(1)} fusion(s32[256]{0:T(256)S(1)} %bitcast.86, s32[256]{0:T(256)S(1)} %and_select_fusion, s32[]{:T(128)} %constant.80.clone.1), kind=kCustom, calls=%fused_computation.66 | custom fusion | bytes 1540 | tf_op jit(solution)/shard_map/scatter | solution.py:92
  13.7 1.2 fusion.21
  15.0 2.1 %gather_fusion = bf16[384,512]{1,0:T(8,128)(2,1)S(1)} fusion(bf16[129,512]{1,0:T(8,128)(2,1)S(1)} %pad_dynamic-slice_fusion, s32[1024]{0:T(1024)S(1)} %pad_clamp_fusion.1), kind=kCustom, calls=%fused_computation | custom fusion | bytes 787968 | tf_op jit(solution)/shard_map/gather | solution.py:100
  17.1 17.9 %all_to_all.10 = bf16[4,96,512]{2,1,0:T(8,128)(2,1)} all-to-all(bf16[4,96,512]{2,1,0:T(8,128)(2,1)S(1)} %bitcast.83), channel_id=1, replica_groups=mesh['grp'=2,'ep'=4,'tp'=4] {'ep'}, dimensions={0} | all-to-all | bytes 786432 | tf_op jit(solution)/shard_map/all_to_all | solution.py:101
  35.1 2.1 %collective-permute-start = (bf16[15,512]{1,0:T(8,128)(2,1)S(1)}, bf16[15,512]{1,0:T(8,128)(2,1)S(1)}, u32[]{:S(2)}, u32[]{:S(2)}) collective-permute-start(bf16[15,512]{1,0:T(8,128)(2,1)S(1)} %slice.43), channel_id=1, source_target_pairs={{0,4},{4,8},{8,12},{1,5},{5,9},{9,13},{2,6},{6,10},{10,14},{3,7},{... | collective-permute-start | bytes 46088 | tf_op jit(solution)/shard_map/ppermute | solution.py:13
  37.2 16.7 %all-gather.2.cloned.1.call-done = bf16[384,2048]{1,0:T(8,128)(2,1)} async-done(((bf16[384,512]{1,0:T(8,128)(2,1)}), bf16[384,2048]{1,0:T(8,128)(2,1)}) %all-gather.2.cloned.1.call-update) | async-done | bytes 1572880 | tf_op jit(solution)/shard_map/all_gather | solution.py:104
  53.9 5.4 %fusion.4 = f32[384,896]{1,0:T(8,128)} fusion(bf16[384,2048]{1,0:T(8,128)(2,1)} %all-gather.2.cloned.1.call-done, bf16[1,2048,896]{2,1,0:T(8,128)(2,1)} %param.19), kind=kOutput, calls=%fused_computation.7 | convolution fusion | flops 1409286144 | bytes 6619136 | tf_op jit(solution)/shard_map/dot_general | solution.py:105
  59.3 8.6 %fusion.9 = bf16[2048,384]{0,1:T(8,128)(2,1)} fusion(bf16[1,896,2048]{2,1,0:T(8,128)(2,1)} %param.21, bf16[384,2048]{1,0:T(8,128)(2,1)} %all-gather.2.cloned.1.call-done, bf16[1,2048,896]{2,1,0:T(8,128)(2,1)} %param.20, f32[384,896]{1,0:T(8,128)} %fusion.4), kind=kOutput, calls=%fused_computation.10 | convolution fusion | flops 2821423104 | bytes 11862016 | tf_op jit(solution)/shard_map/dot_general | solution.py:119
  68.4 0.8 dynamic_slice.10
  69.4 1.5 %fusion.35 = f32[4,128,256]{2,1,0:T(8,128)S(1)} fusion(bf16[16,128,128]{2,1,0:T(8,128)(2,1)} %param.12, s32[]{:T(128)S(6)} %select_n.46, f32[256]{0:T(256)S(1)} %get-tuple-element.2, f32[270,512]{1,0:T(8,128)S(1)} %slice_add_fusion.1, pred[512]{0:T(512)(128)(4,1)S(1)} %broadcast_bitcast_fusion, f32[256]{0:T(256)S(1)} %get-tuple-element.3, ...), kind=kOutput, calls=%fused_computation.42 | convolution fusion | flops 35389440 | bytes 3282948 | tf_op jit(solution)/shard_map/rgc,gcd->rgd/dot_general | solution.py:65
  71.1 1.7 %fusion.12 = bf16[2048,256]{0,1:T(8,128)(2,1)} fusion(bf16[256,512]{0,1:T(8,128)(2,1)S(1)} %fusion.33, bf16[512,2048]{1,0:T(8,128)(2,1)S(1)} %copy-done), kind=kOutput, calls=%fused_computation.12 | convolution fusion | flops 537395200 | bytes 3407872 | tf_op jit(solution)/shard_map/dot_general | solution.py:110
  72.8 23.4 %reduce-scatter.5.cloned.1.call-done = bf16[512,384]{0,1:T(8,128)(2,1)} async-done(((bf16[2048,384]{0,1:T(8,128)(2,1)}), bf16[512,384]{0,1:T(8,128)(2,1)}) %reduce-scatter.5.cloned.1.call-update) | async-done | bytes 393232 | tf_op jit(solution)/shard_map/reduce_scatter | solution.py:118
  96.2 4.6 %all-to-all-start.1 = ((bf16[512,4,96]{0,2,1:T(8,128)(2,1)}), bf16[512,4,96]{0,2,1:T(8,128)(2,1)S(1)}, u32[]{:S(2)}, u32[]{:S(2)}) async-start(bf16[512,4,96]{0,2,1:T(8,128)(2,1)} %bitcast.84), calls=%async_computation.3 | async-start | bytes 786432 | tf_op jit(solution)/shard_map/all_to_all | solution.py:128
  100.9 11.4 %all-to-all-done.1 = bf16[512,4,96]{0,2,1:T(8,128)(2,1)S(1)} async-done(((bf16[512,4,96]{0,2,1:T(8,128)(2,1)}), bf16[512,4,96]{0,2,1:T(8,128)(2,1)S(1)}, u32[]{:S(2)}, u32[]{:S(2)}) %all-to-all-start.1) | async-done | bytes 393248 | tf_op jit(solution)/shard_map/all_to_all | solution.py:128
  112.3 1.2 gather_fusion.1
  113.5 0.3 reshape.150
  113.8 1.4 %multiply_reduce_fusion = bf16[512,128]{0,1:T(8,128)(2,1)} fusion(f32[512,128,2]{0,2,1:T(2,128)S(1)} %reshape.150, f32[128,2]{1,0:T(8,128)S(1)} %copy.25), kind=kLoop, calls=%fused_computation.39 | loop fusion | flops 196608 | bytes 656384 | tf_op jit(solution)/shard_map/reduce_sum | solution.py:133
  115.2 8.9 %reduce-scatter.3.cloned.1.call-done = bf16[512,256]{0,1:T(8,128)(2,1)} async-done(((bf16[2048,256]{0,1:T(8,128)(2,1)}), bf16[512,256]{0,1:T(8,128)(2,1)}) %reduce-scatter.3.cloned.1.call-update) | async-done | bytes 262160 | tf_op jit(solution)/shard_map/reduce_scatter | solution.py:109
  (46 shorter events, 1.8 us)
Async XLA Ops:
  7.2 63.9 %copy-start = (bf16[512,2048]{1,0:T(8,128)(2,1)S(1)}, bf16[512,2048]{1,0:T(8,128)(2,1)}, u32[]{:S(2)}) copy-start(bf16[512,2048]{1,0:T(8,128)(2,1)} %param.14) | copy-start | bytes 6291460
  7.2 46.7 %all-gather.2.cloned.1.call-start = ((), (), s32[]{:S(2)}) async-start(), calls=%async_computation.5 | async-start | bytes 1966080 | tf_op jit(solution)/shard_map/all_gather | solution.py:104
  15.0 20.1 %copy-start.1 = (bf16[256,512]{1,0:T(8,128)(2,1)S(1)}, bf16[256,512]{1,0:T(8,128)(2,1)}, u32[]{:S(2)}) copy-start(bf16[256,512]{1,0:T(8,128)(2,1)} %param.11) | copy-start | bytes 786436
  35.0 61.2 %reduce-scatter.5.cloned.1.call-start = ((), (), s32[]{:S(2)}) async-start(), calls=%async_computation.6 | async-start | bytes 1966080 | tf_op jit(solution)/shard_map/reduce_scatter | solution.py:118
  35.1 34.0 %collective-permute-start = (bf16[15,512]{1,0:T(8,128)(2,1)S(1)}, bf16[15,512]{1,0:T(8,128)(2,1)S(1)}, u32[]{:S(2)}, u32[]{:S(2)}) collective-permute-start(bf16[15,512]{1,0:T(8,128)(2,1)S(1)} %slice.43), channel_id=1, source_target_pairs={{0,4},{4,8},{8,12},{1,5},{5,9},{9,13},{2,6},{6,10},{10,14},{3,7},{... | collective-permute-start | bytes 46088 | tf_op jit(solution)/shard_map/ppermute | solution.py:13
  67.9 56.2 %reduce-scatter.3.cloned.1.call-start = ((), (), s32[]{:S(2)}) async-start(), calls=%async_computation.4 | async-start | bytes 1310720 | tf_op jit(solution)/shard_map/reduce_scatter | solution.py:109
  72.8 28.0 %copy-start.2 = (f32[128,2]{0,1:T(2,128)S(1)}, f32[128,2]{0,1:T(2,128)}, u32[]{:S(2)}) copy-start(f32[128,2]{0,1:T(2,128)} %param.18) | copy-start | bytes 3076
  96.2 16.1 %all-to-all-start.1 = ((bf16[512,4,96]{0,2,1:T(8,128)(2,1)}), bf16[512,4,96]{0,2,1:T(8,128)(2,1)S(1)}, u32[]{:S(2)}, u32[]{:S(2)}) async-start(bf16[512,4,96]{0,2,1:T(8,128)(2,1)} %bitcast.84), calls=%async_computation.3 | async-start | bytes 786432 | tf_op jit(solution)/shard_map/all_to_all | solution.py:128
Sparse Core Ops, SparseCore 0:
  35.1 18.7 all-gather.1
  68.1 28.0 reduce-scatter.4
  99.3 24.7 reduce-scatter.2
where the time goes:
time: 131 us
  waiting for transfers between devices  60.4 us (46%)
  blocking collectives  17.9 us (14%)
  matrix products  17.2 us (13%)
  between operations  14 us (11%)
  local copies, waits for them, and re-layouts  7.86 us (6%)
  starting transfers between devices  6.83 us (5%)
  other arithmetic  6.43 us (5%)
    reduce_scatter x1, waiting for transfers between devices, on_device(): lax.psum_scatter(lax.dot_general(weight_cols, hidden, (((0,), (1,)), ((),...  23.4 us
    all_to_all x1, blocking collectives, on_device(): lax.all_to_all(outgoing, 'ep', split_axis=0, concat_axis=0, tiled=True)  17.9 us
    all_gather x1, waiting for transfers between devices, on_device(): section = lax.all_gather(arrived, 'tp', axis=1, tiled=True)  16.7 us
    all_to_all x1, waiting for transfers between devices, on_device(): lax.all_to_all(results, 'ep', split_axis=1, concat_axis=1, tiled=True)  11.4 us
    reduce_scatter x1, waiting for transfers between devices, on_device(): lax.psum_scatter(lax.dot_general(weight_cols, pooled, (((0,), (1,)), ((),...  8.93 us
    dot_general x1, matrix products, on_device(): lax.dot_general(weight_cols, hidden, (((0,), (1,)), ((), ())), preferred_...  8.61 us
    dot_general x1, matrix products, on_device(): gate_pre = jnp.dot(section, w_gate, preferred_element_type=jnp.float32)  5.4 us
    all_to_all x1, starting transfers between devices, on_device(): lax.all_to_all(results, 'ep', split_axis=1, concat_axis=1, tiled=True)  4.6 us
  transfers between devices with their start and end apart: 5, of which 4 were waited for; matrix products, arithmetic and copies ran while one was open for 17% of the time, Pallas kernels for 0%

commit v1 on v0

--- a/solution.py
+++ b/solution.py
@@ -2,6 +2,7 @@
 import jax.numpy as jnp
 from jax import lax
 from jax.sharding import PartitionSpec as P
+from jax.lax import all_gather
 
 windows = (2, 4, 8, 16)
 epsilon = 1e-06
@@ -101,7 +102,8 @@
     arrived = lax.all_to_all(outgoing, "ep", split_axis=0, concat_axis=0, tiled=True).reshape(
         arrived_rows, columns
     )
-    section = lax.all_gather(arrived, "tp", axis=1, tiled=True)
+    field_out = all_gather(arrived, "tp")
+    section = jnp.concatenate(field_out, axis=1)
     gate_pre = jnp.dot(section, w_gate, preferred_element_type=jnp.float32)
     up_pre = jnp.dot(section, w_up, preferred_element_type=jnp.float32)
     hidden = (jax.nn.silu(gate_pre) * up_pre).astype(jnp.bfloat16)

time: 131 us -> 134 us (1.023)
  local copies, waits for them, and re-layouts: 7.86 us -> 10.4 us
    all_gather x0 -> x1, local copies, waits for them, and re-layouts: none -> 2.59 us  [on_device(): field_out = all_gather(arrived, 'tp')]
  transfers between devices with their start and end apart: 5 -> 5, of which waited for: 4 -> 4; matrix products, arithmetic and copies ran while one was open for 17% -> 18% of each run, Pallas kernels for 0% -> 0%
where the time goes in v1:
time: 134 us; the launch traced here: 133 us
  waiting for transfers between devices  60.4 us (45%)
  blocking collectives  17.9 us (13%)
  matrix products  17.3 us (13%)
  between operations  14 us (10%)
  local copies, waits for them, and re-layouts  10.4 us (8%)
  starting transfers between devices  6.84 us (5%)
  other arithmetic  6.43 us (5%)
    reduce_scatter x1, waiting for transfers between devices, on_device(): lax.psum_scatter(lax.dot_general(weight_cols, hidden, (((0,), (1,)), ((),...  23.4 us
    all_to_all x1, blocking collectives, on_device(): lax.all_to_all(outgoing, 'ep', split_axis=0, concat_axis=0, tiled=True)  17.9 us
    all_gather x1, waiting for transfers between devices, on_device(): field_out = all_gather(arrived, 'tp')  16.7 us
    all_to_all x1, waiting for transfers between devices, on_device(): lax.all_to_all(results, 'ep', split_axis=1, concat_axis=1, tiled=True)  11.4 us
    reduce_scatter x1, waiting for transfers between devices, on_device(): lax.psum_scatter(lax.dot_general(weight_cols, pooled, (((0,), (1,)), ((),...  8.93 us
    dot_general x1, matrix products, on_device(): lax.dot_general(weight_cols, hidden, (((0,), (1,)), ((), ())), preferred_...  8.7 us
    dot_general x1, matrix products, on_device(): gate_pre = jnp.dot(section, w_gate, preferred_element_type=jnp.float32)  5.42 us
    all_to_all x1, starting transfers between devices, on_device(): lax.all_to_all(results, 'ep', split_axis=1, concat_axis=1, tiled=True)  4.6 us
  transfers between devices with their start and end apart: 5, of which 4 were waited for; matrix products, arithmetic and copies ran while one was open for 18% of the time, Pallas kernels for 0%

profile of v1, /device:TPU:0, one launch (start us, length us, event | category | flops | bytes accessed | tf_op | source)
XLA Modules:
  0.0 133.4 jit_solution(10331654955853851028)
XLA Ops:
  7.2 0.9 copy.39
  8.4 0.7 broadcast_multiply_fusion
  9.1 1.2 fusion.19
  10.4 1.2 reduce-window.6
  12.1 0.1 mul.84
  12.3 1.4 %scatter_custom_fusion = s32[384]{0:T(512)S(1)} fusion(s32[256]{0:T(256)S(1)} %bitcast.91, s32[256]{0:T(256)S(1)} %and_select_fusion, s32[]{:T(128)} %constant.80.clone.1), kind=kCustom, calls=%fused_computation.66 | custom fusion | bytes 1540 | tf_op jit(solution)/shard_map/scatter | solution.py:93
  13.7 1.2 fusion.21
  15.0 2.1 %gather_fusion = bf16[384,512]{1,0:T(8,128)(2,1)S(1)} fusion(bf16[129,512]{1,0:T(8,128)(2,1)S(1)} %pad_dynamic-slice_fusion, s32[1024]{0:T(1024)S(1)} %pad_clamp_fusion.1), kind=kCustom, calls=%fused_computation | custom fusion | bytes 787968 | tf_op jit(solution)/shard_map/gather | solution.py:101
  17.1 17.9 %all_to_all.10 = bf16[4,96,512]{2,1,0:T(8,128)(2,1)} all-to-all(bf16[4,96,512]{2,1,0:T(8,128)(2,1)S(1)} %bitcast.88), channel_id=1, replica_groups=mesh['grp'=2,'ep'=4,'tp'=4] {'ep'}, dimensions={0} | all-to-all | bytes 786432 | tf_op jit(solution)/shard_map/all_to_all | solution.py:102
  35.1 2.1 %collective-permute-start = (bf16[15,512]{1,0:T(8,128)(2,1)S(1)}, bf16[15,512]{1,0:T(8,128)(2,1)S(1)}, u32[]{:S(2)}, u32[]{:S(2)}) collective-permute-start(bf16[15,512]{1,0:T(8,128)(2,1)S(1)} %slice.43), channel_id=1, source_target_pairs={{0,4},{4,8},{8,12},{1,5},{5,9},{9,13},{2,6},{6,10},{10,14},{3,7},{... | collective-permute-start | bytes 46088 | tf_op jit(solution)/shard_map/ppermute | solution.py:14
  37.2 16.7 %all-gather.2.cloned.1.call-done = bf16[4,384,512]{2,1,0:T(8,128)(2,1)} async-done(((bf16[1,384,512]{2,1,0:T(8,128)(2,1)}), bf16[4,384,512]{2,1,0:T(8,128)(2,1)}) %all-gather.2.cloned.1.call-update) | async-done | bytes 1572880 | tf_op jit(solution)/shard_map/all_gather | solution.py:105
  53.9 2.6 %copy.43 = bf16[4,384,512]{1,2,0:T(8,128)(2,1)} copy(bf16[4,384,512]{2,1,0:T(8,128)(2,1)} %all-gather.2.cloned.1.call-done) | data formatting | bytes 3145728 | tf_op jit(solution)/shard_map/all_gather | solution.py:105
  56.5 5.4 %fusion.4 = f32[384,896]{1,0:T(8,128)} fusion(bf16[384,2048]{0,1:T(8,128)(2,1)} %bitcast.85, bf16[1,2048,896]{2,1,0:T(8,128)(2,1)} %param.19), kind=kOutput, calls=%fused_computation.7 | convolution fusion | flops 1409286144 | bytes 6619136 | tf_op jit(solution)/shard_map/dot_general | solution.py:107
  61.9 8.7 %fusion.9 = bf16[2048,384]{0,1:T(8,128)(2,1)} fusion(bf16[1,896,2048]{2,1,0:T(8,128)(2,1)} %param.21, bf16[384,2048]{0,1:T(8,128)(2,1)} %bitcast.86, bf16[1,2048,896]{2,1,0:T(8,128)(2,1)} %param.20, f32[384,896]{1,0:T(8,128)} %fusion.4), kind=kOutput, calls=%fused_computation.10 | convolution fusion | flops 2821423104 | bytes 11862016 | tf_op jit(solution)/shard_map/dot_general | solution.py:121
  71.1 0.8 dynamic_slice.10
  72.1 1.5 %fusion.35 = f32[4,128,256]{2,1,0:T(8,128)S(1)} fusion(bf16[16,128,128]{2,1,0:T(8,128)(2,1)} %param.12, s32[]{:T(128)S(6)} %select_n.46, f32[256]{0:T(256)S(1)} %get-tuple-element.2, f32[270,512]{1,0:T(8,128)S(1)} %slice_add_fusion.1, pred[512]{0:T(512)(128)(4,1)S(1)} %broadcast_bitcast_fusion, f32[256]{0:T(256)S(1)} %get-tuple-element.3, ...), kind=kOutput, calls=%fused_computation.42 | convolution fusion | flops 35389440 | bytes 3282948 | tf_op jit(solution)/shard_map/rgc,gcd->rgd/dot_general | solution.py:66
  73.8 1.7 %fusion.12 = bf16[2048,256]{0,1:T(8,128)(2,1)} fusion(bf16[256,512]{0,1:T(8,128)(2,1)S(1)} %fusion.33, bf16[512,2048]{1,0:T(8,128)(2,1)S(1)} %copy-done), kind=kOutput, calls=%fused_computation.12 | convolution fusion | flops 537395200 | bytes 3407872 | tf_op jit(solution)/shard_map/dot_general | solution.py:112
  75.5 23.4 %reduce-scatter.5.cloned.1.call-done = bf16[512,384]{0,1:T(8,128)(2,1)} async-done(((bf16[2048,384]{0,1:T(8,128)(2,1)}), bf16[512,384]{0,1:T(8,128)(2,1)}) %reduce-scatter.5.cloned.1.call-update) | async-done | bytes 393232 | tf_op jit(solution)/shard_map/reduce_scatter | solution.py:120
  98.9 4.6 %all-to-all-start.1 = ((bf16[512,4,96]{0,2,1:T(8,128)(2,1)}), bf16[512,4,96]{0,2,1:T(8,128)(2,1)S(1)}, u32[]{:S(2)}, u32[]{:S(2)}) async-start(bf16[512,4,96]{0,2,1:T(8,128)(2,1)} %bitcast.89), calls=%async_computation.3 | async-start | bytes 786432 | tf_op jit(solution)/shard_map/all_to_all | solution.py:130
  103.6 11.4 %all-to-all-done.1 = bf16[512,4,96]{0,2,1:T(8,128)(2,1)S(1)} async-done(((bf16[512,4,96]{0,2,1:T(8,128)(2,1)}), bf16[512,4,96]{0,2,1:T(8,128)(2,1)S(1)}, u32[]{:S(2)}, u32[]{:S(2)}) %all-to-all-start.1) | async-done | bytes 393248 | tf_op jit(solution)/shard_map/all_to_all | solution.py:130
  115.0 1.2 gather_fusion.1
  116.2 0.3 reshape.154
  116.5 1.4 %multiply_reduce_fusion = bf16[512,128]{0,1:T(8,128)(2,1)} fusion(f32[512,128,2]{0,2,1:T(2,128)S(1)} %reshape.154, f32[128,2]{1,0:T(8,128)S(1)} %copy.44), kind=kLoop, calls=%fused_computation.39 | loop fusion | flops 196608 | bytes 656384 | tf_op jit(solution)/shard_map/reduce_sum | solution.py:135
  117.9 8.9 %reduce-scatter.3.cloned.1.call-done = bf16[512,256]{0,1:T(8,128)(2,1)} async-done(((bf16[2048,256]{0,1:T(8,128)(2,1)}), bf16[512,256]{0,1:T(8,128)(2,1)}) %reduce-scatter.3.cloned.1.call-update) | async-done | bytes 262160 | tf_op jit(solution)/shard_map/reduce_scatter | solution.py:111
  (47 shorter events, 2.0 us)
Async XLA Ops:
  7.2 66.6 %copy-start = (bf16[512,2048]{1,0:T(8,128)(2,1)S(1)}, bf16[512,2048]{1,0:T(8,128)(2,1)}, u32[]{:S(2)}) copy-start(bf16[512,2048]{1,0:T(8,128)(2,1)} %param.14) | copy-start | bytes 6291460
  7.2 46.7 %all-gather.2.cloned.1.call-start = ((), (), s32[]{:S(2)}) async-start(), calls=%async_computation.5 | async-start | bytes 1966080 | tf_op jit(solution)/shard_map/all_gather | solution.py:105
  15.0 20.1 %copy-start.1 = (bf16[256,512]{1,0:T(8,128)(2,1)S(1)}, bf16[256,512]{1,0:T(8,128)(2,1)}, u32[]{:S(2)}) copy-start(bf16[256,512]{1,0:T(8,128)(2,1)} %param.11) | copy-start | bytes 786436
  35.0 63.9 %reduce-scatter.5.cloned.1.call-start = ((), (), s32[]{:S(2)}) async-start(), calls=%async_computation.6 | async-start | bytes 1966080 | tf_op jit(solution)/shard_map/reduce_scatter | solution.py:120
  35.1 36.7 %collective-permute-start = (bf16[15,512]{1,0:T(8,128)(2,1)S(1)}, bf16[15,512]{1,0:T(8,128)(2,1)S(1)}, u32[]{:S(2)}, u32[]{:S(2)}) collective-permute-start(bf16[15,512]{1,0:T(8,128)(2,1)S(1)} %slice.43), channel_id=1, source_target_pairs={{0,4},{4,8},{8,12},{1,5},{5,9},{9,13},{2,6},{6,10},{10,14},{3,7},{... | collective-permute-start | bytes 46088 | tf_op jit(solution)/shard_map/ppermute | solution.py:14
  70.6 56.2 %reduce-scatter.3.cloned.1.call-start = ((), (), s32[]{:S(2)}) async-start(), calls=%async_computation.4 | async-start | bytes 1310720 | tf_op jit(solution)/shard_map/reduce_scatter | solution.py:111
  75.5 28.0 %copy-start.2 = (f32[128,2]{0,1:T(2,128)S(1)}, f32[128,2]{0,1:T(2,128)}, u32[]{:S(2)}) copy-start(f32[128,2]{0,1:T(2,128)} %param.18) | copy-start | bytes 3076
  98.9 16.1 %all-to-all-start.1 = ((bf16[512,4,96]{0,2,1:T(8,128)(2,1)}), bf16[512,4,96]{0,2,1:T(8,128)(2,1)S(1)}, u32[]{:S(2)}, u32[]{:S(2)}) async-start(bf16[512,4,96]{0,2,1:T(8,128)(2,1)} %bitcast.89), calls=%async_computation.3 | async-start | bytes 786432 | tf_op jit(solution)/shard_map/all_to_all | solution.py:130
Sparse Core Ops, SparseCore 0:
  35.1 18.7 all-gather.1
  70.8 28.0 reduce-scatter.4
  102.0 24.7 reduce-scatter.2
